TPU v7x, 32 devices: a whole 2x2x4 slice. The times are simulated.
32 devices in a mesh: sp: 4 (over z), tp: 4 (over y, x), dp: 2 (over core).
Axes of the slice: x: 2, y: 2, z: 4, core: 2. Of those that a mesh axis runs over, the one named last changes fastest.
Arguments:
- latent: bfloat16 [2, 512, 2048], P('dp', ('sp', 'tp')), may hold values from -10 to 10
- condition: bfloat16 [2, 2048], P('dp'), may hold values from -6 to 6
- context: bfloat16 [2, 512, 2048], P('dp', 'sp'), may hold values from -6 to 6
- context_source: bfloat16 [2048], replicated, may hold values from -6 to 6
- mod_weight: bfloat16 [3, 2048, 2048], P(None, 'sp', 'tp'), may hold values from -0.125 to 0.125
- norm_gain: bfloat16 [2048], replicated, may hold values from 0.099609375 to 1.8984375
- w_x: bfloat16 [2048, 2048], P('dp', 'tp'), may hold values from -0.125 to 0.125
- w_b: bfloat16 [2048, 512], P('dp', 'tp'), may hold values from -0.125 to 0.125
- w_c: bfloat16 [2048, 512], P('dp', 'tp'), may hold values from -0.125 to 0.125
- w_z: bfloat16 [2048, 2048], P('dp', 'tp'), may hold values from -0.125 to 0.125
- w_dt: bfloat16 [2, 2048, 32], P(None, 'dp', 'tp'), may hold values from -0.125 to 0.125
- conv_x: bfloat16 [3, 2048], P(None, 'tp'), may hold values from -3.5 to 3.5
- conv_b: bfloat16 [3, 512], P(None, 'tp'), may hold values from -3.5 to 3.5
- conv_c: bfloat16 [3, 512], P(None, 'tp'), may hold values from -3.5 to 3.5
- decay_rate: float32 [2, 32], P(None, 'tp'), may hold values from 0 to 1, as said below
- out_gain: bfloat16 [2048], P('tp'), may hold values from 0.099609375 to 1.8984375
- w_out: bfloat16 [2048, 2048], P(('tp', 'dp')), may hold values from -0.125 to 0.125
Outputs:
- update: bfloat16 [2, 512, 2048], P('dp', ('sp', 'tp'))
Inputs may be any that keep to these rules, and one draw needn't show every extreme that they name: `decay_rate`: positive rates.
All inputs are finite; a program needn't handle non-finite values.
Results may differ from a plain program's by a relative error of at most 0.014.
Values may be sent and summed in bfloat16 or wider, within the bound.
A program may use at most 128 MiB of HBM per device.

v0:
```python
import jax
import jax.numpy as jnp
from jax import lax
from jax.sharding import PartitionSpec as P

STATE = 128
BLOCK = 128
EPSILON = 1e-06


def with_halo(x, sides, width):
    for axis, dim in sides:
        peers, length = (lax.axis_size(axis), x.shape[dim])
        up = [(i, (i + 1) % peers) for i in range(peers - 1)]
        down = [(j, i) for i, j in up]
        last = lax.slice_in_dim(x, length - width, length, axis=dim)
        leading = lax.slice_in_dim(x, 0, width, axis=dim)
        before = lax.ppermute(last, axis, up)
        after = lax.ppermute(leading, axis, down)
        x = jnp.concatenate([before, x, after], axis=dim)
    return x


def carried_in_2(x, axis, combine, identity, reverse):
    peers, place = (lax.axis_size(axis), lax.axis_index(axis))
    everything = jax.tree.map(
        lambda part, kind: lax.all_gather(part.astype(kind), axis), x, (jnp.bfloat16, jnp.bfloat16)
    )
    start = jax.tree.map(
        lambda part, zero: jnp.broadcast_to(jnp.asarray(zero, part.dtype), part.shape), x, identity
    )

    def hop(k, before):
        at = peers - 1 - k if reverse else k
        reached = at > place if reverse else at < place
        new = combine(
            before, jax.tree.map(lambda part, own: part[at].astype(own.dtype), everything, x)
        )
        return jax.tree.map(lambda a, b: jnp.where(reached, a, b), new, before)

    return lax.fori_loop(0, peers, hop, start)


def rounded(values):
    return lax.optimization_barrier(values.astype(jnp.bfloat16)).astype(jnp.float32)


def modulated(source, gain_vec, shift_vec, scale_vec):
    values = source.astype(jnp.float32)
    normed = values * lax.rsqrt(jnp.mean(values * values, axis=-1, keepdims=True) + EPSILON)
    return (normed * gain_vec.astype(jnp.float32) * (1.0 + scale_vec) + shift_vec).astype(
        jnp.bfloat16
    )


def convolved(padded, weight, total_rows):
    wide_vals = padded.astype(jnp.float32)
    tap_weights = weight.astype(jnp.float32)
    summed = jnp.zeros((total_rows, wide_vals.shape[1]), jnp.float32)
    for offset in range(weight.shape[0]):
        summed = summed + wide_vals[offset : offset + total_rows] * tap_weights[offset]
    return jax.nn.silu(summed).astype(jnp.bfloat16)


def final_state(x_vals, b_vals, step_size, rate_head, groups):
    total_rows, head_count = step_size.shape
    per_group = head_count // groups
    moved_x = rounded(
        x_vals.reshape(total_rows, head_count, -1).astype(jnp.float32) * step_size[:, :, None]
    )
    running = jnp.cumsum(-rate_head * step_size, axis=0)
    weight = jnp.exp(running[-1:] - running)
    scaled = (moved_x * weight[:, :, None]).reshape(total_rows, groups, per_group, -1)
    b_wide = b_vals.reshape(total_rows, groups, -1).astype(jnp.float32)
    ctx_state = jnp.einsum("sgn,sghp->ghpn", b_wide, scaled, precision=lax.Precision.HIGHEST)
    return (ctx_state, running[-1].reshape(groups, per_group))


def combine_states(earlier, later_part):
    return (
        earlier[0] + later_part[0],
        earlier[1] * jnp.exp(later_part[0])[:, :, None, None] + later_part[1],
    )


def direction_terms(x_vals, b_vals, c_vals, step_size, rate_head, groups):
    total_rows, head_count = step_size.shape
    per_group = head_count // groups
    blocks = total_rows // BLOCK
    moved_x = (
        x_vals.reshape(total_rows, head_count, -1).astype(jnp.float32) * step_size[:, :, None]
    ).astype(jnp.bfloat16)
    head_dim = moved_x.shape[2]
    x_blocks = moved_x.reshape(blocks, BLOCK, groups, per_group, head_dim)
    b_blocks = b_vals.reshape(blocks, BLOCK, groups, -1)
    c_blocks = c_vals.reshape(blocks, BLOCK, groups, -1)
    running = jnp.cumsum((-rate_head * step_size).reshape(blocks, BLOCK, head_count), axis=1)
    across = jnp.swapaxes(running, 1, 2)
    spread = across[:, :, :, None] - across[:, :, None, :]
    lower_part = lax.broadcasted_iota(jnp.int32, (BLOCK, BLOCK), 0) >= lax.broadcasted_iota(
        jnp.int32, (BLOCK, BLOCK), 1
    )
    decay_mask = jnp.where(lower_part, jnp.exp(jnp.minimum(spread, 0.0)), 0.0).reshape(
        blocks, groups, per_group, BLOCK, BLOCK
    )
    scores = jnp.einsum("clgn,csgn->cgls", c_blocks, b_blocks, preferred_element_type=jnp.float32)
    weights = (scores[:, :, None] * decay_mask).astype(jnp.bfloat16)
    inside = jnp.einsum("cghls,csghp->clghp", weights, x_blocks, preferred_element_type=jnp.float32)
    to_end = jnp.exp(running[:, -1:, :] - running).reshape(blocks, BLOCK, groups, per_group, 1)
    x_end = (x_blocks.astype(jnp.float32) * to_end).astype(jnp.bfloat16)
    fresh_state = jnp.einsum(
        "csgn,csghp->cghpn", b_blocks, x_end, preferred_element_type=jnp.float32
    )
    totals = running[:, -1, :].reshape(blocks, groups, per_group)

    def advance(carried_in, inputs):
        return (carried_in * jnp.exp(inputs[1])[:, :, None, None] + inputs[0], carried_in)

    ending, before = lax.scan(
        advance, jnp.zeros(fresh_state.shape[1:], jnp.float32), (fresh_state, totals)
    )
    return (inside, before, ending, totals, running, c_blocks)


def direction_output(terms, incoming):
    inside, before, ending, totals, running, c_blocks = terms
    blocks, length, groups, per_group, head_dim = inside.shape
    offset_sum = jnp.cumsum(totals, axis=0) - totals
    entering = before + jnp.exp(offset_sum)[:, :, :, None, None] * incoming[None]
    carried = jnp.einsum(
        "clgn,cghpn->clghp",
        c_blocks,
        entering.astype(jnp.bfloat16),
        preferred_element_type=jnp.float32,
    )
    growth = jnp.exp(running).reshape(blocks, length, groups, per_group, 1)
    return (inside + growth * carried).reshape(blocks * length, -1)


def shards(
    latent,
    condition,
    context,
    context_source,
    mod_weight,
    norm_gain,
    w_x,
    w_b,
    w_c,
    w_z,
    w_dt,
    conv_x,
    conv_b,
    conv_c,
    decay_rate,
    out_gain,
    w_out,
):
    row_count = mod_weight.shape[1]
    activations = jnp.stack(
        [
            jax.nn.silu(condition[0].astype(jnp.float32)),
            jax.nn.silu(context_source.astype(jnp.float32)),
        ]
    ).astype(jnp.bfloat16)
    own_rows = lax.dynamic_slice_in_dim(activations, lax.axis_index("sp") * row_count, row_count, 1)
    partial_value = jnp.einsum(
        "ar,krc->kac", own_rows, mod_weight, preferred_element_type=jnp.float32
    )
    summed = lax.psum(partial_value, "sp")
    mod_vectors = lax.all_gather(summed, "tp", axis=2, tiled=True)
    full_x, full_b, full_c, full_z, full_fwd, full_bwd, full_out = (
        lax.all_gather(w_x, "dp", axis=0, tiled=True),
        lax.all_gather(w_b, "dp", axis=0, tiled=True),
        lax.all_gather(w_c, "dp", axis=0, tiled=True),
        lax.all_gather(w_z, "dp", axis=0, tiled=True),
        lax.all_gather(w_dt[0], "dp", axis=0, tiled=True),
        lax.all_gather(w_dt[1], "dp", axis=0, tiled=True),
        lax.all_gather(w_out, "dp", axis=0, tiled=True),
    )
    inner_cols = full_x.shape[1]
    gn_cols = full_b.shape[1]
    head_count = full_fwd.shape[1]
    groups = gn_cols // STATE
    mixed_cols = inner_cols + gn_cols
    reach_rows = conv_x.shape[0] // 2
    rate_fwd = decay_rate[0]
    rate_bwd = decay_rate[1]
    all_weights = jnp.concatenate([full_x, full_b, full_c, full_fwd, full_bwd, full_z], axis=1)
    ctx_weight = jnp.concatenate([full_x, full_b, full_fwd, full_bwd], axis=1)
    taps_all = jnp.concatenate([conv_x, conv_b, conv_c], axis=1)
    ctx_taps = jnp.concatenate([conv_x, conv_b], axis=1)
    ctx_rows = modulated(context[0], norm_gain, mod_vectors[0, 1], mod_vectors[1, 1])
    own_features = jnp.dot(ctx_rows, ctx_weight, preferred_element_type=jnp.float32).astype(
        jnp.bfloat16
    )
    own_count = own_features.shape[0]
    padded = with_halo(own_features[:, :mixed_cols], (("sp", 0),), reach_rows)
    smoothed = convolved(padded, ctx_taps, own_count)
    step_size = jax.nn.softplus(own_features[:, mixed_cols:].astype(jnp.float32))
    ctx_x = smoothed[:, :inner_cols]
    ctx_b = smoothed[:, inner_cols:]
    part_fwd, total_fwd = final_state(ctx_x, ctx_b, step_size[:, :head_count], rate_fwd, groups)
    part_bwd, total_bwd = final_state(
        jnp.flip(ctx_x, 0),
        jnp.flip(ctx_b, 0),
        jnp.flip(step_size[:, head_count:], 0),
        rate_bwd,
        groups,
    )
    totals = lax.all_gather(jnp.stack([total_fwd, total_bwd])[None], "sp", axis=0, tiled=True)
    device_order = jnp.arange(totals.shape[0])
    own_index = lax.axis_index("sp")
    after_sum = jnp.sum(
        jnp.where((device_order > own_index)[:, None, None], totals[:, 0], 0.0), axis=0
    )
    before_sum = jnp.sum(
        jnp.where((device_order < own_index)[:, None, None], totals[:, 1], 0.0), axis=0
    )
    ctx_fwd, ctx_bwd = lax.psum(
        (
            part_fwd * jnp.exp(after_sum)[:, :, None, None],
            part_bwd * jnp.exp(before_sum)[:, :, None, None],
        ),
        "sp",
    )
    latent_rows = modulated(latent[0], norm_gain, mod_vectors[0, 0], mod_vectors[1, 0])
    features = jnp.dot(
        lax.all_gather(latent_rows, "tp", axis=0, tiled=True),
        all_weights,
        preferred_element_type=jnp.float32,
    ).astype(jnp.bfloat16)
    total_rows = features.shape[0]
    padded = with_halo(features[:, : mixed_cols + gn_cols], (("sp", 0),), reach_rows)
    smoothed = convolved(padded, taps_all, total_rows)
    x_vals = smoothed[:, :inner_cols]
    b_vals = smoothed[:, inner_cols:mixed_cols]
    c_vals = smoothed[:, mixed_cols:]
    base_col = mixed_cols + gn_cols
    step_size = jax.nn.softplus(
        features[:, base_col : base_col + 2 * head_count].astype(jnp.float32)
    )
    gate_in = features[:, base_col + 2 * head_count :]
    forward_terms = direction_terms(
        x_vals, b_vals, c_vals, step_size[:, :head_count], rate_fwd, groups
    )
    backward_terms = direction_terms(
        jnp.flip(x_vals, 0),
        jnp.flip(b_vals, 0),
        jnp.flip(c_vals, 0),
        jnp.flip(step_size[:, head_count:], 0),
        rate_bwd,
        groups,
    )
    fwd_total = jnp.sum(forward_terms[3], axis=0)
    bwd_total = jnp.sum(backward_terms[3], axis=0)
    empty = (jnp.zeros_like(fwd_total), jnp.zeros_like(forward_terms[2]))
    prefix_decay, prefix_state = carried_in_2(
        (fwd_total, forward_terms[2]), "sp", combine_states, empty, False
    )
    suffix_decay, suffix_state = carried_in_2(
        (bwd_total, backward_terms[2]), "sp", combine_states, empty, True
    )
    out_fwd = direction_output(
        forward_terms, prefix_state + jnp.exp(prefix_decay)[:, :, None, None] * ctx_fwd
    )
    out_bwd = jnp.flip(
        direction_output(
            backward_terms, suffix_state + jnp.exp(suffix_decay)[:, :, None, None] * ctx_bwd
        ),
        0,
    )
    gated = (out_fwd + out_bwd) * jax.nn.silu(gate_in.astype(jnp.float32))
    grouped = gated.reshape(total_rows, groups, -1)
    normed = (
        grouped
        * lax.rsqrt(jnp.mean(grouped * grouped, axis=-1, keepdims=True) + EPSILON)
        * out_gain.reshape(groups, -1).astype(jnp.float32)
    )
    normed_out = normed.reshape(total_rows, -1).astype(jnp.bfloat16)
    mixed = lax.psum_scatter(
        jnp.dot(normed_out, full_out, preferred_element_type=jnp.float32).astype(jnp.bfloat16),
        "tp",
        scatter_dimension=0,
        tiled=True,
    ).astype(jnp.float32)
    return (mod_vectors[2, 0] * mixed).astype(jnp.bfloat16)[None]


def solution(mesh):
    placed = (
        P("dp", ("sp", "tp"), None),
        P("dp", None),
        P("dp", "sp", None),
        P(),
        P(None, "sp", "tp"),
        P(),
        P("dp", "tp"),
        P("dp", "tp"),
        P("dp", "tp"),
        P("dp", "tp"),
        P(None, "dp", "tp"),
        P(None, "tp"),
        P(None, "tp"),
        P(None, "tp"),
        P(None, "tp"),
        P("tp"),
        P(("tp", "dp"), None),
    )
    return jax.shard_map(
        shards, mesh=mesh, in_specs=placed, out_specs=P("dp", ("sp", "tp"), None), check_vma=False
    )
```

profile of v0, /device:TPU:0, one launch (start us, length us, event | category | flops | bytes accessed | tf_op | source)
XLA Modules:
  0.0 216.8 jit_solution(12759376264633219292)
XLA Ops:
  9.9 20.4 %psum.21 = f32[3,2,512]{2,1,0:T(2,128)S(1)} all-reduce(f32[3,2,512]{2,1,0:T(2,128)S(1)} %convolution_bitcast_fusion.4), channel_id=1, replica_groups=mesh['sp'=4,'tp'=4,'dp'=2] {'sp'}, use_global_device_ids=true, to_apply=%region_0.1 | all-reduce | flops 3072 | bytes 24576 | tf_op jit(solution)/shard_map/psum | solution.py:170
  30.4 8.3 %all_gather.50 = f32[3,2,2048]{2,1,0:T(2,128)S(1)} all-gather(f32[3,2,512]{2,1,0:T(2,128)S(1)} %psum.21), channel_id=1, replica_groups=mesh['sp'=4,'tp'=4,'dp'=2] {'tp'}, dimensions={2}, use_global_device_ids=true | all-gather | bytes 61440 | tf_op jit(solution)/shard_map/all_gather | solution.py:171
  39.1 1.8 all-gather
  41.2 1.8 all-gather.1
  43.3 10.0 %all_gather.51 = bf16[128,2048]{1,0:T(8,128)(2,1)S(1)} all-gather(bf16[32,2048]{1,0:T(8,128)(2,1)S(1)} %fusion.46), channel_id=1, replica_groups=mesh['sp'=4,'tp'=4,'dp'=2] {'tp'}, dimensions={0}, use_global_device_ids=true | all-gather | bytes 655360 | tf_op jit(solution)/shard_map/all_gather | solution.py:229
  53.9 3.8 %all_gather.53 = bf16[2048,128]{1,0:T(8,128)(2,1)} all-gather(bf16[1024,128]{1,0:T(8,128)(2,1)} %param.28), channel_id=1, replica_groups=mesh['sp'=4,'tp'=4,'dp'=2] {'dp'}, dimensions={0}, use_global_device_ids=true | all-gather | bytes 786432 | tf_op jit(solution)/shard_map/all_gather | solution.py:174
  57.7 4.1 %all_gather.54 = bf16[2048,128]{1,0:T(8,128)(2,1)} all-gather(bf16[1024,128]{1,0:T(8,128)(2,1)} %param.29), channel_id=1, replica_groups=mesh['sp'=4,'tp'=4,'dp'=2] {'dp'}, dimensions={0}, use_global_device_ids=true | all-gather | bytes 786432 | tf_op jit(solution)/shard_map/all_gather | solution.py:175
  61.8 1.2 fusion.23
  63.0 3.5 %fusion.16 = bf16[128,656]{0,1:T(8,128)(2,1)S(1)} fusion(bf16[2048,8]{1,0:T(8,128)(2,1)S(1)} %copy.71, bf16[2048,8]{1,0:T(8,128)(2,1)S(1)} %copy.70, bf16[2048,128]{1,0:T(8,128)(2,1)} %all_gather.53, bf16[2048,512]{1,0:T(8,128)(2,1)} %all-gather.9.cloned.1.call-done, bf16[1,128,2048]{2,1,0:T(8,128)(2,1)} %param.23, f32[2048]{0:T(1024)S(1)} %bitcast.220, ...), kind=kOutput, calls=%fused_computation.38 | convolution fusion | flops 356337664 | bytes 3404288 | tf_op jit(solution)/shard_map/dot_general | solution.py:194
  67.4 10.2 %concatenate.18 = bf16[2048,1296]{1,0:T(8,128)(2,1)} concatenate(bf16[2048,512]{1,0:T(8,128)(2,1)} %all-gather.9.cloned.1.call-done, bf16[2048,128]{1,0:T(8,128)(2,1)} %all_gather.53, bf16[2048,128]{1,0:T(8,128)(2,1)} %all_gather.54, bf16[2048,8]{1,0:T(8,128)(2,1)S(1)} %copy.70, bf16[2048,8]{1,0:T(8,128)(2,1)S(1)} %copy.71, bf16[2048,512]{1,0:T(8,128)(2,1)} %all-gather.11.cloned.1.call-done), dimensions={1} | concatenate | bytes 10616832 | tf_op jit(solution)/shard_map/concatenate | solution.py:189
  77.6 5.0 %convolution_convert_fusion.1 = bf16[128,1296]{0,1:T(8,128)(2,1)S(1)} fusion(bf16[128,2048]{1,0:T(8,128)(2,1)S(1)} %all_gather.51, bf16[2048,1296]{1,0:T(8,128)(2,1)} %concatenate.18), kind=kOutput, calls=%fused_computation.23 | convolution fusion | flops 679643136 | bytes 6164480 | tf_op jit(solution)/shard_map/dot_general | solution.py:228
  84.0 7.6 %all-gather.3 = f32[8,1,8]{2,1,0:T(1,128)S(1)} all-gather(f32[2,1,8]{2,1,0:T(1,128)S(1)} %pad_maximum_fusion.3), channel_id=5, replica_groups=mesh['sp'=4,'tp'=4,'dp'=2] {'sp'}, dimensions={0}, use_global_device_ids=true | all-gather | bytes 320 | tf_op jit(solution)/shard_map/all_gather | solution.py:211
  91.7 3.9 %collective-permute-start.2 = (bf16[1,640]{0,1:T(8,128)(2,1)S(1)}, bf16[1,640]{0,1:T(8,128)(2,1)S(1)}, u32[]{:S(2)}, u32[]{:S(2)}) collective-permute-start(bf16[1,640]{0,1:T(8,128)(2,1)S(1)} %copy-done.5), channel_id=1, source_target_pairs={{0,8},{8,16},{16,24},{1,9},{9,17},{17,25},{2,10},{10,18},{18,26},{... | collective-permute-start | bytes 3848 | tf_op jit(solution)/shard_map/ppermute | solution.py:18
  95.6 1.3 collective-permute-start.3
  97.2 1.1 collective-permute-done.2
  98.4 4.4 %collective-permute-done.3 = bf16[1,640]{0,1:T(8,128)(2,1)S(1)} collective-permute-done((bf16[1,640]{0,1:T(8,128)(2,1)S(1)}, bf16[1,640]{0,1:T(8,128)(2,1)S(1)}, u32[]{:S(2)}, u32[]{:S(2)}) %collective-permute-start.3) | collective-permute-done | bytes 1312 | tf_op jit(solution)/shard_map/ppermute | solution.py:19
  104.1 1.0 fusion.14
  105.1 1.0 fusion.12
  111.0 1.9 collective-permute-start
  113.0 1.3 collective-permute-start.1
  116.1 11.0 %all_gather.58 = bf16[4,1,8]{2,1,0:T(2,128)(2,1)} all-gather(bf16[1,1,8]{2,1,0:T(2,128)(2,1)S(1)} %slice.299), channel_id=1, replica_groups=mesh['sp'=4,'tp'=4,'dp'=2] {'sp'}, dimensions={0}, use_global_device_ids=true | all-gather | bytes 80 | tf_op jit(solution)/shard_map/all_gather | solution.py:27
  127.2 10.0 %all_gather.62 = bf16[4,1,8]{2,1,0:T(2,128)(2,1)} all-gather(bf16[1,1,8]{2,1,0:T(2,128)(2,1)S(1)} %slice.298), channel_id=1, replica_groups=mesh['sp'=4,'tp'=4,'dp'=2] {'sp'}, dimensions={0}, use_global_device_ids=true | all-gather | bytes 80 | tf_op jit(solution)/shard_map/all_gather | solution.py:27
  138.8 1.3 multiply_convert_fusion.2
  141.1 15.0 %all-gather.2 = bf16[32,64,128]{2,1,0:T(8,128)(2,1)S(1)} all-gather(bf16[8,64,128]{2,1,0:T(8,128)(2,1)S(1)} %fusion.21), channel_id=4, replica_groups=mesh['sp'=4,'tp'=4,'dp'=2] {'sp'}, dimensions={0}, use_global_device_ids=true | all-gather | bytes 655360 | tf_op jit(solution)/shard_map/all_gather | solution.py:27
  158.3 15.8 %all-gather.4 = bf16[32,64,128]{2,1,0:T(8,128)(2,1)S(1)} all-gather(bf16[8,64,128]{2,1,0:T(8,128)(2,1)S(1)} %fusion.22), channel_id=6, replica_groups=mesh['sp'=4,'tp'=4,'dp'=2] {'sp'}, dimensions={0}, use_global_device_ids=true | all-gather | bytes 655360 | tf_op jit(solution)/shard_map/all_gather | solution.py:27
  176.4 1.2 fusion.20
  177.6 1.2 fusion.13
  179.2 1.2 fusion.19
  180.4 1.2 fusion.15
  181.8 3.0 %convolution_convert_fusion = bf16[128,2048]{1,0:T(8,128)(2,1)} fusion(bf16[512,2048]{1,0:T(8,128)(2,1)} %all-gather.13.cloned.1.call-done, f32[128,512]{0,1:T(8,128)S(1)} %get-tuple-element.415, f32[512]{0:T(512)} %convert_element_type.388, f32[128]{0:T(128)S(1)} %add_rsqrt_fusion), kind=kOutput, calls=%fused_computation.22 | convolution fusion | flops 268894208 | bytes 2886144 | tf_op jit(solution)/shard_map/dot_general | solution.py:282
  184.8 23.9 %reduce-scatter.2.cloned.1.call-done = bf16[32,2048]{1,0:T(8,128)(2,1)} async-done(((bf16[128,2048]{1,0:T(8,128)(2,1)}), bf16[32,2048]{1,0:T(8,128)(2,1)}) %reduce-scatter.2.cloned.1.call-update) | async-done | bytes 131088 | tf_op jit(solution)/shard_map/reduce_scatter | solution.py:281
  208.7 1.6 fusion.71
  (183 shorter events, 23.9 us)
Async XLA Ops:
  6.5 3.0 %copy-start = (bf16[3,512,512]{2,1,0:T(8,128)(2,1)S(1)}, bf16[3,512,512]{2,1,0:T(8,128)(2,1)}, u32[]{:S(2)}) copy-start(bf16[3,512,512]{2,1,0:T(8,128)(2,1)} %param.25) | copy-start | bytes 4718596
  6.5 32.2 %copy-start.16 = (bf16[2048]{0:T(1024)(128)(2,1)S(1)}, bf16[2048]{0:T(1024)(128)(2,1)}, u32[]{:S(2)}) copy-start(bf16[2048]{0:T(1024)(128)(2,1)} %param.26) | copy-start | bytes 12292
  6.5 32.2 %copy-start.2 = (bf16[1,32,2048]{2,1,0:T(8,128)(2,1)S(1)}, bf16[1,32,2048]{2,1,0:T(8,128)(2,1)}, u32[]{:S(2)}) copy-start(bf16[1,32,2048]{2,1,0:T(8,128)(2,1)} %param.21) | copy-start | bytes 393220
  6.5 32.5 %copy-start.6 = (bf16[2,1024,8]{1,2,0:T(8,128)(2,1)S(1)}, bf16[2,1024,8]{1,2,0:T(8,128)(2,1)}, u32[]{:S(2)}) copy-start(bf16[2,1024,8]{1,2,0:T(8,128)(2,1)} %param.31) | copy-start | bytes 98308
  6.5 36.8 %copy-start.11 = (bf16[3,512]{1,0:T(4,128)(2,1)S(1)}, bf16[3,512]{1,0:T(4,128)(2,1)}, u32[]{:S(2)}) copy-start(bf16[3,512]{1,0:T(4,128)(2,1)} %param.32) | copy-start | bytes 9220
  6.5 36.8 %copy-start.17 = (bf16[3,128]{1,0:T(4,128)(2,1)S(1)}, bf16[3,128]{1,0:T(4,128)(2,1)}, u32[]{:S(2)}) copy-start(bf16[3,128]{1,0:T(4,128)(2,1)} %param.33) | copy-start | bytes 2308
  6.6 56.5 %all-gather.9.cloned.1.call-start = ((), (), s32[]{:S(2)}) async-start(), calls=%async_computation.1 | async-start | bytes 3145728 | tf_op jit(solution)/shard_map/all_gather | solution.py:173
  7.3 60.1 %all-gather.11.cloned.1.call-start = ((), (), s32[]{:S(2)}) async-start(), calls=%async_computation.2 | async-start | bytes 3145728 | tf_op jit(solution)/shard_map/all_gather | solution.py:176
  8.0 168.4 %all-reduce.3.cloned.1.call-start = ((), (), s32[]{:S(2)}) async-start(), calls=%async_computation.5 | async-start | bytes 1048576 | tf_op jit(solution)/shard_map/psum | solution.py:220
  8.8 54.2 %copy-start.20 = (f32[2,8]{1,0:T(2,128)S(1)}, f32[2,8]{1,0:T(2,128)}, u32[]{:S(2)}) copy-start(f32[2,8]{1,0:T(2,128)} %param.35) | copy-start | bytes 196
  77.5 14.1 %copy-start.5 = (bf16[1,640]{0,1:T(8,128)(2,1)S(1)}, bf16[1,640]{0,1:T(8,128)(2,1)}, u32[]{:S(2)}) copy-start(bf16[1,640]{0,1:T(8,128)(2,1)} %get-tuple-element.422) | copy-start | bytes 3844
  77.5 18.0 %copy-start.4 = (bf16[1,640]{0,1:T(8,128)(2,1)S(1)}, bf16[1,640]{0,1:T(8,128)(2,1)}, u32[]{:S(2)}) copy-start(bf16[1,640]{0,1:T(8,128)(2,1)} %get-tuple-element.423) | copy-start | bytes 3844
  77.5 19.4 %copy-start.24 = (pred[4]{0:T(512)(128)(4,1)S(1)}, pred[4]{0:T(512)(128)(4,1)}, u32[]{:S(2)}) copy-start(pred[4]{0:T(512)(128)(4,1)} %get-tuple-element.456) | copy-start | bytes 16
  77.6 25.3 %slice-start = ((bf16[128,656]{0,1:T(8,128)(2,1)}), bf16[128,640]{0,1:T(8,128)(2,1)S(1)}, s32[]{:S(2)}) async-start(bf16[128,656]{0,1:T(8,128)(2,1)} %copy-done.1), calls=%async_computation.6 | async-start | bytes 327680 | tf_op jit(solution)/shard_map/slice | solution.py:198
  91.7 6.7 %collective-permute-start.2 = (bf16[1,640]{0,1:T(8,128)(2,1)S(1)}, bf16[1,640]{0,1:T(8,128)(2,1)S(1)}, u32[]{:S(2)}, u32[]{:S(2)}) collective-permute-start(bf16[1,640]{0,1:T(8,128)(2,1)S(1)} %copy-done.5), channel_id=1, source_target_pairs={{0,8},{8,16},{16,24},{1,9},{9,17},{17,25},{2,10},{10,18},{18,26},{... | collective-permute-start | bytes 3848 | tf_op jit(solution)/shard_map/ppermute | solution.py:18
  95.6 7.2 %collective-permute-start.3 = (bf16[1,640]{0,1:T(8,128)(2,1)S(1)}, bf16[1,640]{0,1:T(8,128)(2,1)S(1)}, u32[]{:S(2)}, u32[]{:S(2)}) collective-permute-start(bf16[1,640]{0,1:T(8,128)(2,1)S(1)} %copy-done.4), channel_id=1, source_target_pairs={{8,0},{16,8},{24,16},{9,1},{17,9},{25,17},{10,2},{18,10},{26,18},{... | collective-permute-start | bytes 3848 | tf_op jit(solution)/shard_map/ppermute | solution.py:19
  97.1 10.3 %copy-start.18 = (bf16[3,128]{1,0:T(4,128)(2,1)S(1)}, bf16[3,128]{1,0:T(4,128)(2,1)}, u32[]{:S(2)}) copy-start(bf16[3,128]{1,0:T(4,128)(2,1)} %param.34) | copy-start | bytes 2308
  97.1 10.9 %copy-start.19 = (bf16[512]{0:T(512)(128)(2,1)S(1)}, bf16[512]{0:T(512)(128)(2,1)}, u32[]{:S(2)}) copy-start(bf16[512]{0:T(512)(128)(2,1)} %param.36) | copy-start | bytes 3076
  106.2 75.6 %all-gather.13.cloned.1.call-start = ((), (), s32[]{:S(2)}) async-start(), calls=%async_computation.3 | async-start | bytes 3145728 | tf_op jit(solution)/shard_map/all_gather | solution.py:179
  106.7 102.0 %reduce-scatter.2.cloned.1.call-start = ((), (), s32[]{:S(2)}) async-start(), calls=%async_computation.4 | async-start | bytes 655360 | tf_op jit(solution)/shard_map/reduce_scatter | solution.py:281
  111.0 27.5 %collective-permute-start = (bf16[1,768]{0,1:T(8,128)(2,1)S(1)}, bf16[1,768]{0,1:T(8,128)(2,1)S(1)}, u32[]{:S(2)}, u32[]{:S(2)}) collective-permute-start(bf16[1,768]{0,1:T(8,128)(2,1)S(1)} %get-tuple-element.416), channel_id=1, source_target_pairs={{0,8},{8,16},{16,24},{1,9},{9,17},{17,25},{2,10},{10,18},{18,26},{... | collective-permute-start | bytes 4616 | tf_op jit(solution)/shard_map/ppermute | solution.py:18
  113.0 25.5 %collective-permute-start.1 = (bf16[1,768]{0,1:T(8,128)(2,1)S(1)}, bf16[1,768]{0,1:T(8,128)(2,1)S(1)}, u32[]{:S(2)}, u32[]{:S(2)}) collective-permute-start(bf16[1,768]{0,1:T(8,128)(2,1)S(1)} %get-tuple-element.417), channel_id=1, source_target_pairs={{8,0},{16,8},{24,16},{9,1},{17,9},{25,17},{10,2},{18,10},{26,18},{... | collective-permute-start | bytes 4616 | tf_op jit(solution)/shard_map/ppermute | solution.py:19
  137.8 3.1 %copy-start.23 = (f32[8]{0:T(128)S(1)}, f32[8]{0:T(128)}, u32[]{:S(2)}) copy-start(f32[8]{0:T(128)} %exponential_multiply_fusion.1) | copy-start | bytes 100
  138.8 17.4 %copy-start.13 = (f32[1,8]{1,0:T(1,128)S(1)}, f32[1,8]{1,0:T(1,128)}, u32[]{:S(2)}) copy-start(f32[1,8]{1,0:T(1,128)} %custom-call) | copy-start | bytes 100
  138.8 17.4 %copy-start.15 = (bf16[4,1,8]{2,1,0:T(2,128)(2,1)S(1)}, bf16[4,1,8]{2,1,0:T(2,128)(2,1)}, u32[]{:S(2)}) copy-start(bf16[4,1,8]{2,1,0:T(2,128)(2,1)} %all_gather.58) | copy-start | bytes 196
  140.1 17.9 %copy-start.8 = (f32[128,8]{0,1:T(8,128)S(1)}, f32[128,8]{0,1:T(8,128)}, u32[]{:S(2)}) copy-start(f32[128,8]{0,1:T(8,128)} %get-tuple-element.448) | copy-start | bytes 12292
  140.1 18.0 %copy-start.22 = (f32[8]{0:T(128)S(1)}, f32[8]{0:T(128)}, u32[]{:S(2)}) copy-start(f32[8]{0:T(128)} %exponential_multiply_fusion) | copy-start | bytes 100
  140.8 33.2 %copy-start.12 = (f32[1,8]{1,0:T(1,128)S(1)}, f32[1,8]{1,0:T(1,128)}, u32[]{:S(2)}) copy-start(f32[1,8]{1,0:T(1,128)} %custom-call.2) | copy-start | bytes 100
  140.8 33.2 %copy-start.14 = (bf16[4,1,8]{2,1,0:T(2,128)(2,1)S(1)}, bf16[4,1,8]{2,1,0:T(2,128)(2,1)}, u32[]{:S(2)}) copy-start(bf16[4,1,8]{2,1,0:T(2,128)(2,1)} %all_gather.62) | copy-start | bytes 196
  156.8 19.6 %copy-start.7 = (f32[128,8]{0,1:T(8,128)S(1)}, f32[128,8]{0,1:T(8,128)}, u32[]{:S(2)}) copy-start(f32[128,8]{0,1:T(8,128)} %get-tuple-element.447) | copy-start | bytes 12292
  156.8 19.6 %copy-start.21 = (f32[8]{0:T(128)S(1)}, f32[8]{0:T(128)}, u32[]{:S(2)}) copy-start(f32[8]{0:T(128)} %get-tuple-element.426) | copy-start | bytes 100
  174.8 5.7 %copy-start.3 = (f32[128,512]{0,1:T(8,128)S(1)}, f32[128,512]{0,1:T(8,128)}, u32[]{:S(2)}) copy-start(f32[128,512]{0,1:T(8,128)} %get-tuple-element.418) | copy-start | bytes 786436
  (3 other events, 6.8 us)
Sparse Core Ops, SparseCore 0:
  8.9 13.3 all-gather.8
  23.8 11.7 all-gather.10
  106.3 40.7 all-reduce.2
  148.5 10.0 all-gather.12
  184.9 23.7 reduce-scatter.1
where the time goes:
time: 218 us; the launch traced here: 217 us
  blocking collectives  110 us (50%)
  waiting for transfers between devices  31.4 us (14%)
  matrix products  20.7 us (9%)
  other arithmetic  16.4 us (8%)
  local copies, waits for them, and re-layouts  15.9 us (7%)
  between operations  13.8 us (6%)
  starting transfers between devices  8.63 us (4%)
    all_gather x4, blocking collectives, carried_in_2(): lax.all_gather(part.astype(kind), axis)  51.8 us
    reduce_scatter x1, waiting for transfers between devices, shards(): lax.psum_scatter(jnp.dot(normed_out, full_out, preferred_element_type=jnp...  23.9 us
    psum x1, blocking collectives, shards(): summed = lax.psum(partial_value, 'sp')  20.4 us
    concatenate x1, local copies, waits for them, and re-layouts, shards(): jnp.concatenate([full_x, full_b, full_c, full_fwd, full_bwd, full_z], axi...  10.2 us
    all_gather x1, blocking collectives, shards(): lax.all_gather(latent_rows, 'tp', axis=0, tiled=True)  10 us
    all_gather x1, blocking collectives, shards(): mod_vectors = lax.all_gather(summed, 'tp', axis=2, tiled=True)  8.34 us
    all_gather x1, blocking collectives, shards(): lax.all_gather(jnp.stack([total_fwd, total_bwd])[None], 'sp', axis=0, til...  7.58 us
    ppermute x2, starting transfers between devices, with_halo(): before = lax.ppermute(last, axis, up)  5.86 us
  transfers between devices with their start and end apart: 9, of which 3 were waited for; matrix products, arithmetic and copies ran while one was open for 13% of the time, Pallas kernels for 0%

commit v1 on v0

--- a/solution.py
+++ b/solution.py
@@ -167,7 +167,9 @@
     partial_value = jnp.einsum(
         "ar,krc->kac", own_rows, mod_weight, preferred_element_type=jnp.float32
     )
-    summed = lax.psum(partial_value, "sp")
+    summed = partial_value
+    for hop_ in (1, 2):
+        summed = summed + lax.ppermute(summed, "sp", [(dev, dev ^ hop_) for dev in range(4)])
     mod_vectors = lax.all_gather(summed, "tp", axis=2, tiled=True)
     full_x, full_b, full_c, full_z, full_fwd, full_bwd, full_out = (
         lax.all_gather(w_x, "dp", axis=0, tiled=True),

time: 218 us -> 198 us (0.908)
  blocking collectives: 110 us -> 85.3 us
  starting transfers between devices: 8.63 us -> 13.9 us
    psum x1 -> x0, blocking collectives: 20.4 us -> none  [shards(): summed = lax.psum(partial_value, 'sp')]
    ppermute x0 -> x2, starting transfers between devices: none -> 5.71 us  [shards(): lax.ppermute(summed, 'sp', [(dev, dev ^ hop_) for dev in range(4)])]
  transfers between devices with their start and end apart: 9 -> 11, of which waited for: 3 -> 3; matrix products, arithmetic and copies ran while one was open for 13% -> 15% of each run, Pallas kernels for 0% -> 0%
where the time goes in v1:
time: 198 us; the launch traced here: 197 us
  blocking collectives  85.3 us (43%)
  waiting for transfers between devices  30.5 us (15%)
  matrix products  20.8 us (11%)
  local copies, waits for them, and re-layouts  17.4 us (9%)
  other arithmetic  15.5 us (8%)
  starting transfers between devices  13.9 us (7%)
  between operations  13.7 us (7%)
    all_gather x4, blocking collectives, carried_in_2(): lax.all_gather(part.astype(kind), axis)  50.4 us
    reduce_scatter x1, waiting for transfers between devices, shards(): lax.psum_scatter(jnp.dot(normed_out, full_out, preferred_element_type=jnp...  23.7 us
    all_gather x1, blocking collectives, shards(): lax.all_gather(latent_rows, 'tp', axis=0, tiled=True)  10.5 us
    concatenate x1, local copies, waits for them, and re-layouts, shards(): jnp.concatenate([full_x, full_b, full_c, full_fwd, full_bwd, full_z], axi...  10.2 us
    all_gather x1, blocking collectives, shards(): mod_vectors = lax.all_gather(summed, 'tp', axis=2, tiled=True)  8.39 us
    all_gather x1, blocking collectives, shards(): lax.all_gather(jnp.stack([total_fwd, total_bwd])[None], 'sp', axis=0, til...  8.01 us
    ppermute x2, starting transfers between devices, shards(): lax.ppermute(summed, 'sp', [(dev, dev ^ hop_) for dev in range(4)])  5.71 us
    ppermute x2, starting transfers between devices, with_halo(): before = lax.ppermute(last, axis, up)  5.42 us
  transfers between devices with their start and end apart: 11, of which 3 were waited for; matrix products, arithmetic and copies ran while one was open for 15% of the time, Pallas kernels for 0%

profile of v1, /device:TPU:0, one launch (start us, length us, event | category | flops | bytes accessed | tf_op | source)
XLA Modules:
  0.0 197.4 jit_solution(15170654587870261484)
XLA Ops:
  9.3 3.1 %collective-permute-start = (f32[3,2,512]{2,1,0:T(2,128)S(1)}, f32[3,2,512]{2,1,0:T(2,128)S(1)}, u32[]{:S(2)}, u32[]{:S(2)}) collective-permute-start(f32[3,2,512]{2,1,0:T(2,128)S(1)} %convolution_bitcast_fusion.4), channel_id=1, source_target_pairs={{0,8},{8,0},{16,24},{24,16},{1,9},{9,1},{17,25},{25,17},{2,10},{10... | collective-permute-start | bytes 36872 | tf_op jit(solution)/shard_map/ppermute | solution.py:172
  12.6 2.2 %all_gather.53 = bf16[2048,128]{1,0:T(8,128)(2,1)S(1)} all-gather(bf16[1024,128]{1,0:T(8,128)(2,1)S(1)} %copy-done.4), channel_id=1, replica_groups=mesh['sp'=4,'tp'=4,'dp'=2] {'dp'}, dimensions={0}, use_global_device_ids=true | all-gather | bytes 786432 | tf_op jit(solution)/shard_map/all_gather | solution.py:176
  15.0 2.2 %all_gather.54 = bf16[2048,128]{1,0:T(8,128)(2,1)S(1)} all-gather(bf16[1024,128]{1,0:T(8,128)(2,1)S(1)} %copy-done.5), channel_id=1, replica_groups=mesh['sp'=4,'tp'=4,'dp'=2] {'dp'}, dimensions={0}, use_global_device_ids=true | all-gather | bytes 786432 | tf_op jit(solution)/shard_map/all_gather | solution.py:177
  17.7 2.7 %collective-permute-start.1 = (f32[3,2,512]{2,1,0:T(2,128)S(1)}, f32[3,2,512]{2,1,0:T(2,128)S(1)}, u32[]{:S(2)}, u32[]{:S(2)}) collective-permute-start(f32[3,2,512]{2,1,0:T(2,128)S(1)} %add.248), channel_id=1, source_target_pairs={{0,16},{8,24},{16,0},{24,8},{1,17},{9,25},{17,1},{25,9},{2,18},{10... | collective-permute-start | bytes 36872 | tf_op jit(solution)/shard_map/ppermute | solution.py:172
  20.3 1.8 all-gather
  22.2 1.0 copy.70
  23.2 1.8 all-gather.1
  25.0 1.0 copy.71
  26.1 8.4 %all_gather.50 = f32[3,2,2048]{2,1,0:T(2,128)S(1)} all-gather(f32[3,2,512]{2,1,0:T(2,128)S(1)} %add.249), channel_id=1, replica_groups=mesh['sp'=4,'tp'=4,'dp'=2] {'tp'}, dimensions={2}, use_global_device_ids=true | all-gather | bytes 61440 | tf_op jit(solution)/shard_map/all_gather | solution.py:173
  34.6 10.5 %all_gather.51 = bf16[128,2048]{1,0:T(8,128)(2,1)S(1)} all-gather(bf16[32,2048]{1,0:T(8,128)(2,1)S(1)} %fusion.46), channel_id=1, replica_groups=mesh['sp'=4,'tp'=4,'dp'=2] {'tp'}, dimensions={0}, use_global_device_ids=true | all-gather | bytes 655360 | tf_op jit(solution)/shard_map/all_gather | solution.py:231
  45.1 3.7 %fusion.16 = bf16[128,656]{0,1:T(8,128)(2,1)S(1)} fusion(bf16[2048,8]{1,0:T(8,128)(2,1)} %copy.71, bf16[2048,8]{1,0:T(8,128)(2,1)} %copy.70, bf16[2048,128]{1,0:T(8,128)(2,1)S(1)} %all_gather.53, bf16[2048,512]{1,0:T(8,128)(2,1)} %all-gather.9.cloned.1.call-done, bf16[1,128,2048]{2,1,0:T(8,128)(2,1)} %param.23, f32[2048]{0:T(1024)S(1)} %bitcast.220, ...), kind=kOutput, calls=%fused_computation.38 | convolution fusion | flops 356337664 | bytes 3404288 | tf_op jit(solution)/shard_map/dot_general | solution.py:196
  49.6 10.2 %concatenate.18 = bf16[2048,1296]{1,0:T(8,128)(2,1)} concatenate(bf16[2048,512]{1,0:T(8,128)(2,1)} %all-gather.9.cloned.1.call-done, bf16[2048,128]{1,0:T(8,128)(2,1)S(1)} %all_gather.53, bf16[2048,128]{1,0:T(8,128)(2,1)S(1)} %all_gather.54, bf16[2048,8]{1,0:T(8,128)(2,1)} %copy.70, bf16[2048,8]{1,0:T(8,128)(2,1)} %copy.71, bf16[2048,512]{1,0:T(8,128)(2,1)} %all-gather.11.cloned.1.call-done), dimensions={1} | concatenate | bytes 10616832 | tf_op jit(solution)/shard_map/concatenate | solution.py:191
  59.8 5.0 %convolution_convert_fusion.1 = bf16[128,1296]{0,1:T(8,128)(2,1)S(1)} fusion(bf16[128,2048]{1,0:T(8,128)(2,1)S(1)} %all_gather.51, bf16[2048,1296]{1,0:T(8,128)(2,1)} %concatenate.18), kind=kOutput, calls=%fused_computation.23 | convolution fusion | flops 679643136 | bytes 6164480 | tf_op jit(solution)/shard_map/dot_general | solution.py:230
  66.3 8.0 %all-gather.3 = f32[8,1,8]{2,1,0:T(1,128)S(1)} all-gather(f32[2,1,8]{2,1,0:T(1,128)S(1)} %pad_maximum_fusion.3), channel_id=5, replica_groups=mesh['sp'=4,'tp'=4,'dp'=2] {'sp'}, dimensions={0}, use_global_device_ids=true | all-gather | bytes 320 | tf_op jit(solution)/shard_map/all_gather | solution.py:213
  74.3 3.5 %collective-permute-start.4 = (bf16[1,640]{0,1:T(8,128)(2,1)S(1)}, bf16[1,640]{0,1:T(8,128)(2,1)S(1)}, u32[]{:S(2)}, u32[]{:S(2)}) collective-permute-start(bf16[1,640]{0,1:T(8,128)(2,1)S(1)} %copy-done.8), channel_id=1, source_target_pairs={{0,8},{8,16},{16,24},{1,9},{9,17},{17,25},{2,10},{10,18},{18,26},{... | collective-permute-start | bytes 3848 | tf_op jit(solution)/shard_map/ppermute | solution.py:18
  77.9 1.3 collective-permute-start.5
  79.5 1.1 collective-permute-done.4
  80.7 4.4 %collective-permute-done.5 = bf16[1,640]{0,1:T(8,128)(2,1)S(1)} collective-permute-done((bf16[1,640]{0,1:T(8,128)(2,1)S(1)}, bf16[1,640]{0,1:T(8,128)(2,1)S(1)}, u32[]{:S(2)}, u32[]{:S(2)}) %collective-permute-start.5) | collective-permute-done | bytes 1312 | tf_op jit(solution)/shard_map/ppermute | solution.py:19
  93.3 1.9 collective-permute-start.2
  95.2 1.3 collective-permute-start.3
  98.4 10.7 %all_gather.58 = bf16[4,1,8]{2,1,0:T(2,128)(2,1)} all-gather(bf16[1,1,8]{2,1,0:T(2,128)(2,1)S(1)} %slice.299), channel_id=1, replica_groups=mesh['sp'=4,'tp'=4,'dp'=2] {'sp'}, dimensions={0}, use_global_device_ids=true | all-gather | bytes 80 | tf_op jit(solution)/shard_map/all_gather | solution.py:27
  109.1 8.0 %all_gather.62 = bf16[4,1,8]{2,1,0:T(2,128)(2,1)} all-gather(bf16[1,1,8]{2,1,0:T(2,128)(2,1)S(1)} %slice.298), channel_id=1, replica_groups=mesh['sp'=4,'tp'=4,'dp'=2] {'sp'}, dimensions={0}, use_global_device_ids=true | all-gather | bytes 80 | tf_op jit(solution)/shard_map/all_gather | solution.py:27
  118.7 1.3 multiply_convert_fusion.2
  121.0 17.0 %all-gather.2 = bf16[32,64,128]{2,1,0:T(8,128)(2,1)S(1)} all-gather(bf16[8,64,128]{2,1,0:T(8,128)(2,1)S(1)} %fusion.21), channel_id=4, replica_groups=mesh['sp'=4,'tp'=4,'dp'=2] {'sp'}, dimensions={0}, use_global_device_ids=true | all-gather | bytes 655360 | tf_op jit(solution)/shard_map/all_gather | solution.py:27
  140.2 14.8 %all-gather.4 = bf16[32,64,128]{2,1,0:T(8,128)(2,1)S(1)} all-gather(bf16[8,64,128]{2,1,0:T(8,128)(2,1)S(1)} %fusion.22), channel_id=6, replica_groups=mesh['sp'=4,'tp'=4,'dp'=2] {'sp'}, dimensions={0}, use_global_device_ids=true | all-gather | bytes 655360 | tf_op jit(solution)/shard_map/all_gather | solution.py:27
  157.3 1.2 fusion.20
  158.5 1.2 fusion.13
  160.1 1.2 fusion.19
  161.3 1.2 fusion.15
  162.7 3.0 %convolution_convert_fusion = bf16[128,2048]{1,0:T(8,128)(2,1)} fusion(bf16[512,2048]{1,0:T(8,128)(2,1)} %all-gather.13.cloned.1.call-done, f32[128,512]{0,1:T(8,128)S(1)} %get-tuple-element.415, f32[512]{0:T(512)} %convert_element_type.388, f32[128]{0:T(128)S(1)} %add_rsqrt_fusion), kind=kOutput, calls=%fused_computation.22 | convolution fusion | flops 268894208 | bytes 2886144 | tf_op jit(solution)/shard_map/dot_general | solution.py:284
  165.7 23.7 %reduce-scatter.2.cloned.1.call-done = bf16[32,2048]{1,0:T(8,128)(2,1)} async-done(((bf16[128,2048]{1,0:T(8,128)(2,1)}), bf16[32,2048]{1,0:T(8,128)(2,1)}) %reduce-scatter.2.cloned.1.call-update) | async-done | bytes 131088 | tf_op jit(solution)/shard_map/reduce_scatter | solution.py:283
  189.3 1.6 fusion.71
  (194 shorter events, 25.0 us)
Async XLA Ops:
  6.5 6.0 %copy-start.4 = (bf16[1024,128]{1,0:T(8,128)(2,1)S(1)}, bf16[1024,128]{1,0:T(8,128)(2,1)}, u32[]{:S(2)}) copy-start(bf16[1024,128]{1,0:T(8,128)(2,1)} %param.28) | copy-start | bytes 786436
  6.5 8.2 %copy-start.23 = (f32[2,8]{1,0:T(2,128)S(1)}, f32[2,8]{1,0:T(2,128)}, u32[]{:S(2)}) copy-start(f32[2,8]{1,0:T(2,128)} %param.35) | copy-start | bytes 196
  6.5 8.2 %copy-start.2 = (bf16[1,128,2048]{2,1,0:T(8,128)(2,1)S(1)}, bf16[1,128,2048]{2,1,0:T(8,128)(2,1)}, u32[]{:S(2)}) copy-start(bf16[1,128,2048]{2,1,0:T(8,128)(2,1)} %param.23) | copy-start | bytes 1572868
  6.6 8.4 %copy-start.5 = (bf16[1024,128]{1,0:T(8,128)(2,1)S(1)}, bf16[1024,128]{1,0:T(8,128)(2,1)}, u32[]{:S(2)}) copy-start(bf16[1024,128]{1,0:T(8,128)(2,1)} %param.29) | copy-start | bytes 786436
  6.6 15.6 %copy-start.19 = (bf16[2048]{0:T(1024)(128)(2,1)S(1)}, bf16[2048]{0:T(1024)(128)(2,1)}, u32[]{:S(2)}) copy-start(bf16[2048]{0:T(1024)(128)(2,1)} %param.26) | copy-start | bytes 12292
  6.6 38.6 %all-gather.9.cloned.1.call-start = ((), (), s32[]{:S(2)}) async-start(), calls=%async_computation.1 | async-start | bytes 3145728 | tf_op jit(solution)/shard_map/all_gather | solution.py:175
  7.3 18.7 %copy-start.14 = (bf16[3,512]{1,0:T(4,128)(2,1)S(1)}, bf16[3,512]{1,0:T(4,128)(2,1)}, u32[]{:S(2)}) copy-start(bf16[3,512]{1,0:T(4,128)(2,1)} %param.32) | copy-start | bytes 9220
  7.3 18.7 %copy-start.20 = (bf16[3,128]{1,0:T(4,128)(2,1)S(1)}, bf16[3,128]{1,0:T(4,128)(2,1)}, u32[]{:S(2)}) copy-start(bf16[3,128]{1,0:T(4,128)(2,1)} %param.33) | copy-start | bytes 2308
  7.3 42.3 %all-gather.11.cloned.1.call-start = ((), (), s32[]{:S(2)}) async-start(), calls=%async_computation.2 | async-start | bytes 3145728 | tf_op jit(solution)/shard_map/all_gather | solution.py:178
  9.3 8.4 %collective-permute-start = (f32[3,2,512]{2,1,0:T(2,128)S(1)}, f32[3,2,512]{2,1,0:T(2,128)S(1)}, u32[]{:S(2)}, u32[]{:S(2)}) collective-permute-start(f32[3,2,512]{2,1,0:T(2,128)S(1)} %convolution_bitcast_fusion.4), channel_id=1, source_target_pairs={{0,8},{8,0},{16,24},{24,16},{1,9},{9,1},{17,25},{25,17},{2,10},{10... | collective-permute-start | bytes 36872 | tf_op jit(solution)/shard_map/ppermute | solution.py:172
  12.3 145.0 %all-reduce.3.cloned.1.call-start = ((), (), s32[]{:S(2)}) async-start(), calls=%async_computation.5 | async-start | bytes 1048576 | tf_op jit(solution)/shard_map/psum | solution.py:222
  17.7 8.4 %collective-permute-start.1 = (f32[3,2,512]{2,1,0:T(2,128)S(1)}, f32[3,2,512]{2,1,0:T(2,128)S(1)}, u32[]{:S(2)}, u32[]{:S(2)}) collective-permute-start(f32[3,2,512]{2,1,0:T(2,128)S(1)} %add.248), channel_id=1, source_target_pairs={{0,16},{8,24},{16,0},{24,8},{1,17},{9,25},{17,1},{25,9},{2,18},{10... | collective-permute-start | bytes 36872 | tf_op jit(solution)/shard_map/ppermute | solution.py:172
  59.8 14.5 %copy-start.8 = (bf16[1,640]{0,1:T(8,128)(2,1)S(1)}, bf16[1,640]{0,1:T(8,128)(2,1)}, u32[]{:S(2)}) copy-start(bf16[1,640]{0,1:T(8,128)(2,1)} %get-tuple-element.422) | copy-start | bytes 3844
  59.8 18.1 %copy-start.7 = (bf16[1,640]{0,1:T(8,128)(2,1)S(1)}, bf16[1,640]{0,1:T(8,128)(2,1)}, u32[]{:S(2)}) copy-start(bf16[1,640]{0,1:T(8,128)(2,1)} %get-tuple-element.423) | copy-start | bytes 3844
  59.8 19.4 %copy-start.27 = (pred[4]{0:T(512)(128)(4,1)S(1)}, pred[4]{0:T(512)(128)(4,1)}, u32[]{:S(2)}) copy-start(pred[4]{0:T(512)(128)(4,1)} %get-tuple-element.456) | copy-start | bytes 16
  59.8 25.3 %slice-start = ((bf16[128,656]{0,1:T(8,128)(2,1)}), bf16[128,640]{0,1:T(8,128)(2,1)S(1)}, s32[]{:S(2)}) async-start(bf16[128,656]{0,1:T(8,128)(2,1)} %copy-done.1), calls=%async_computation.6 | async-start | bytes 327680 | tf_op jit(solution)/shard_map/slice | solution.py:200
  74.3 6.3 %collective-permute-start.4 = (bf16[1,640]{0,1:T(8,128)(2,1)S(1)}, bf16[1,640]{0,1:T(8,128)(2,1)S(1)}, u32[]{:S(2)}, u32[]{:S(2)}) collective-permute-start(bf16[1,640]{0,1:T(8,128)(2,1)S(1)} %copy-done.8), channel_id=1, source_target_pairs={{0,8},{8,16},{16,24},{1,9},{9,17},{17,25},{2,10},{10,18},{18,26},{... | collective-permute-start | bytes 3848 | tf_op jit(solution)/shard_map/ppermute | solution.py:18
  77.9 7.2 %collective-permute-start.5 = (bf16[1,640]{0,1:T(8,128)(2,1)S(1)}, bf16[1,640]{0,1:T(8,128)(2,1)S(1)}, u32[]{:S(2)}, u32[]{:S(2)}) collective-permute-start(bf16[1,640]{0,1:T(8,128)(2,1)S(1)} %copy-done.7), channel_id=1, source_target_pairs={{8,0},{16,8},{24,16},{9,1},{17,9},{25,17},{10,2},{18,10},{26,18},{... | collective-permute-start | bytes 3848 | tf_op jit(solution)/shard_map/ppermute | solution.py:19
  79.4 10.3 %copy-start.21 = (bf16[3,128]{1,0:T(4,128)(2,1)S(1)}, bf16[3,128]{1,0:T(4,128)(2,1)}, u32[]{:S(2)}) copy-start(bf16[3,128]{1,0:T(4,128)(2,1)} %param.34) | copy-start | bytes 2308
  79.4 10.9 %copy-start.22 = (bf16[512]{0:T(512)(128)(2,1)S(1)}, bf16[512]{0:T(512)(128)(2,1)}, u32[]{:S(2)}) copy-start(bf16[512]{0:T(512)(128)(2,1)} %param.36) | copy-start | bytes 3076
  88.4 74.3 %all-gather.13.cloned.1.call-start = ((), (), s32[]{:S(2)}) async-start(), calls=%async_computation.3 | async-start | bytes 3145728 | tf_op jit(solution)/shard_map/all_gather | solution.py:181
  89.0 100.3 %reduce-scatter.2.cloned.1.call-start = ((), (), s32[]{:S(2)}) async-start(), calls=%async_computation.4 | async-start | bytes 655360 | tf_op jit(solution)/shard_map/reduce_scatter | solution.py:283
  93.3 25.1 %collective-permute-start.2 = (bf16[1,768]{0,1:T(8,128)(2,1)S(1)}, bf16[1,768]{0,1:T(8,128)(2,1)S(1)}, u32[]{:S(2)}, u32[]{:S(2)}) collective-permute-start(bf16[1,768]{0,1:T(8,128)(2,1)S(1)} %get-tuple-element.416), channel_id=1, source_target_pairs={{0,8},{8,16},{16,24},{1,9},{9,17},{17,25},{2,10},{10,18},{18,26},{... | collective-permute-start | bytes 4616 | tf_op jit(solution)/shard_map/ppermute | solution.py:18
  95.2 23.2 %collective-permute-start.3 = (bf16[1,768]{0,1:T(8,128)(2,1)S(1)}, bf16[1,768]{0,1:T(8,128)(2,1)S(1)}, u32[]{:S(2)}, u32[]{:S(2)}) collective-permute-start(bf16[1,768]{0,1:T(8,128)(2,1)S(1)} %get-tuple-element.417), channel_id=1, source_target_pairs={{8,0},{16,8},{24,16},{9,1},{17,9},{25,17},{10,2},{18,10},{26,18},{... | collective-permute-start | bytes 4616 | tf_op jit(solution)/shard_map/ppermute | solution.py:19
  118.7 19.4 %copy-start.16 = (f32[1,8]{1,0:T(1,128)S(1)}, f32[1,8]{1,0:T(1,128)}, u32[]{:S(2)}) copy-start(f32[1,8]{1,0:T(1,128)} %custom-call) | copy-start | bytes 100
  118.7 19.3 %copy-start.18 = (bf16[4,1,8]{2,1,0:T(2,128)(2,1)S(1)}, bf16[4,1,8]{2,1,0:T(2,128)(2,1)}, u32[]{:S(2)}) copy-start(bf16[4,1,8]{2,1,0:T(2,128)(2,1)} %all_gather.58) | copy-start | bytes 196
  120.0 19.9 %copy-start.11 = (f32[128,8]{0,1:T(8,128)S(1)}, f32[128,8]{0,1:T(8,128)}, u32[]{:S(2)}) copy-start(f32[128,8]{0,1:T(8,128)} %get-tuple-element.448) | copy-start | bytes 12292
  120.0 19.9 %copy-start.25 = (f32[8]{0:T(128)S(1)}, f32[8]{0:T(128)}, u32[]{:S(2)}) copy-start(f32[8]{0:T(128)} %exponential_multiply_fusion) | copy-start | bytes 100
  120.8 34.2 %copy-start.15 = (f32[1,8]{1,0:T(1,128)S(1)}, f32[1,8]{1,0:T(1,128)}, u32[]{:S(2)}) copy-start(f32[1,8]{1,0:T(1,128)} %custom-call.2) | copy-start | bytes 100
  120.8 34.2 %copy-start.17 = (bf16[4,1,8]{2,1,0:T(2,128)(2,1)S(1)}, bf16[4,1,8]{2,1,0:T(2,128)(2,1)}, u32[]{:S(2)}) copy-start(bf16[4,1,8]{2,1,0:T(2,128)(2,1)} %all_gather.62) | copy-start | bytes 196
  138.7 18.6 %copy-start.10 = (f32[128,8]{0,1:T(8,128)S(1)}, f32[128,8]{0,1:T(8,128)}, u32[]{:S(2)}) copy-start(f32[128,8]{0,1:T(8,128)} %get-tuple-element.447) | copy-start | bytes 12292
  138.7 18.6 %copy-start.24 = (f32[8]{0:T(128)S(1)}, f32[8]{0:T(128)}, u32[]{:S(2)}) copy-start(f32[8]{0:T(128)} %get-tuple-element.426) | copy-start | bytes 100
  (8 other events, 29.7 us)
Sparse Core Ops, SparseCore 0:
  8.9 13.2 all-gather.8
  23.8 11.7 all-gather.10
  88.5 39.7 all-reduce.2
  129.7 9.8 all-gather.12
  165.8 23.4 reduce-scatter.1
